TPU v7x, 32 devices: a whole 2x2x4 slice. The times are simulated.
32 devices in a mesh: sp: 8 (over z, core), tp: 4 (over y, x).
Axes of the slice: x: 2, y: 2, z: 4, core: 2. Of those that a mesh axis runs over, the one named last changes fastest.
Arguments:
- queries: bfloat16 [4096, 1024], P('sp', 'tp'), may hold values from -20 to 20
- key_vectors: bfloat16 [4096, 1024], P('sp', 'tp'), may hold values from -20 to 20
- value_vectors: bfloat16 [4096, 1024], P('sp', 'tp'), may hold values from -6 to 6
- log_gate_sums: float32 [4096, 16], P('sp', 'tp'), may hold values from -588 to 0, as said below
- residual: bfloat16 [4096, 2048], P('sp', 'tp'), may hold values from -24 to 24
- out_weight: bfloat16 [1024, 2048], P(None, 'tp'), may hold values from -0.75 to 0.75
- norm_gain: bfloat16 [2048], replicated, may hold values from 0.099609375 to 1.8984375
- routes: int32 [4096, 2], P('sp'), may hold values from 0 to 31, all different within a row; in each aligned block of 512 rows (0 to 511, 512 to 1023, ...) at most 40 rows name the same one
- route_weight: float32 [4096, 2], P('sp'), may hold values from 0.5 to 1.5
- expert_gate: bfloat16 [32, 2048, 512], P('sp', None, 'tp'), may hold values from -0.125 to 0.125
- expert_up: bfloat16 [32, 2048, 512], P('sp', None, 'tp'), may hold values from -0.125 to 0.125
- expert_down: bfloat16 [32, 512, 2048], P('sp', None, 'tp'), may hold values from -0.25 to 0.25
- shared_gate: bfloat16 [2048, 512], P(None, 'tp'), may hold values from -0.125 to 0.125
- shared_up: bfloat16 [2048, 512], P(None, 'tp'), may hold values from -0.125 to 0.125
- shared_down: bfloat16 [512, 2048], P(None, 'tp'), may hold values from -0.25 to 0.25
Outputs:
- layer_out: bfloat16 [4096, 2048], P('sp', 'tp')
Inputs may be any that keep to these rules, and one draw needn't show every extreme that they name: `log_gate_sums`: for each head the values do not rise along the positions. `routes`: each row names 2 different experts; among the rows of one index of sp no expert is named by more than 40 rows, a bound that some block reaches.
All inputs are finite; a program needn't handle non-finite values.
Results may differ from a plain program's by a relative error of at most 0.014.
Values may be sent and summed in bfloat16 or wider, within the bound.
A program may use at most 64 MiB of HBM per device.

v0:
```python
import math
import jax
import jax.numpy as jnp
from jax import lax
from jax.sharding import PartitionSpec as P

HDIM = 64
EPSILON = 1e-06


def silu_gate(gate_part, up_part):
    return jax.nn.silu(gate_part) * up_part


def slot_targets(routes, experts_all, capacity):
    flat_routes = routes.reshape(-1)
    onehot = (flat_routes[:, None] == jnp.arange(experts_all, dtype=jnp.int32)[None, :]).astype(
        jnp.int32
    )
    before = jnp.cumsum(onehot, axis=0) - onehot
    return flat_routes * capacity + jnp.sum(before * onehot, axis=1)


def keep_state(fold_state):
    return fold_state


def shards(
    queries,
    key_vectors,
    value_vectors,
    log_gate_sums,
    residual,
    out_weight,
    norm_gain,
    routes,
    route_weight,
    expert_gate,
    expert_up,
    expert_down,
    shared_gate,
    shared_up,
    shared_down,
):
    tok_dev = queries.shape[0]
    head_dim = HDIM
    local_heads = log_gate_sums.shape[1]
    local_width = residual.shape[1]
    model_width = norm_gain.shape[0]
    score_scale = head_dim ** (-0.5)
    seq_first = lax.axis_index("sp") * tok_dev
    query_heads = queries.reshape(tok_dev, local_heads, head_dim)
    query_pos = seq_first + jnp.arange(tok_dev, dtype=jnp.int32)
    own_gates = log_gate_sums.T
    all_gates = lax.all_gather(log_gate_sums, "sp", axis=0, tiled=True)
    initial = (
        jnp.full((local_heads, tok_dev), -1e30, jnp.float32),
        jnp.zeros((local_heads, tok_dev), jnp.float32),
        jnp.zeros((local_heads, tok_dev, head_dim), jnp.float32),
    )
    key_heads = key_vectors.reshape(tok_dev, local_heads, head_dim)
    value_heads = value_vectors.reshape(tok_dev, local_heads, head_dim)
    key_part = lax.all_gather(key_heads, "sp", axis=0, tiled=True)
    value_part = lax.all_gather(value_heads, "sp", axis=0, tiled=True)
    part_rows = key_part.shape[0]
    block_size = math.gcd(part_rows, 512)
    key_blocks = key_part.reshape(part_rows // block_size, block_size, local_heads, head_dim)
    value_blocks = value_part.reshape(part_rows // block_size, block_size, local_heads, head_dim)

    def one_block(fold_state, inputs):
        key_block, value_block, block_number = inputs
        block_first = block_number * block_size

        def compute(old_state):
            running_max, weight_total, summed = old_state
            gate_block = lax.dynamic_slice_in_dim(all_gates, block_first, block_size, 0).T
            scores = (
                jnp.einsum(
                    "qhd,khd->hqk", query_heads, key_block, preferred_element_type=jnp.float32
                )
                * score_scale
            )
            scores = scores + own_gates[:, :, None] - gate_block[:, None, :]
            key_pos = block_first + jnp.arange(block_size, dtype=jnp.int32)
            allowed = (key_pos[None, :] <= query_pos[:, None])[None]
            newmax = jnp.maximum(running_max, jnp.max(jnp.where(allowed, scores, -jnp.inf), axis=2))
            factor = jnp.exp(running_max - newmax)
            weight = jnp.where(allowed, jnp.exp(scores - newmax[:, :, None]), 0.0)
            weight_total = weight_total * factor + jnp.sum(weight, axis=2)
            summed = summed * factor[:, :, None] + jnp.einsum(
                "hqk,khd->hqd",
                weight.astype(jnp.bfloat16),
                value_block,
                preferred_element_type=jnp.float32,
            )
            return (newmax, weight_total, summed)

        useful = block_first <= seq_first + tok_dev - 1
        return (lax.cond(useful, compute, keep_state, fold_state), None)

    numbers = jnp.arange(part_rows // block_size, dtype=jnp.int32)
    result_state, _ = lax.scan(one_block, initial, (key_blocks, value_blocks, numbers))
    running_max, weight_total, summed = result_state
    attended = (summed / weight_total[:, :, None]).astype(jnp.bfloat16)
    attended = attended.transpose(1, 0, 2).reshape(tok_dev, local_heads * head_dim)
    weight_rows = out_weight
    projected = jnp.dot(
        lax.all_gather(attended, "tp", axis=1, tiled=True),
        weight_rows,
        preferred_element_type=jnp.float32,
    )
    mid = (residual.astype(jnp.float32) + projected).astype(jnp.bfloat16)
    mid_wide = mid.astype(jnp.float32)
    feature_first = lax.axis_index("tp") * local_width
    squares = lax.psum(jnp.sum(mid_wide * mid_wide, axis=1), "tp")
    inverse = lax.rsqrt(squares / model_width + EPSILON)
    own_gain = lax.dynamic_slice_in_dim(norm_gain, feature_first, local_width, 0).astype(
        jnp.float32
    )
    normed_own = (mid_wide * inverse[:, None] * own_gain[None, :]).astype(jnp.bfloat16)
    normed = lax.all_gather(normed_own, "tp", axis=1, tiled=True)
    shared_mid = silu_gate(
        jnp.dot(normed, shared_gate, preferred_element_type=jnp.float32),
        jnp.dot(normed, shared_up, preferred_element_type=jnp.float32),
    ).astype(jnp.bfloat16)
    weight_rows = shared_down
    shared_out = jnp.dot(
        lax.all_gather(shared_mid, "tp", axis=1, tiled=True),
        weight_rows,
        preferred_element_type=jnp.float32,
    )
    exp_dev = expert_gate.shape[0]
    sp_count = lax.axis_size("sp")
    experts_all = exp_dev * sp_count
    top_count = routes.shape[1]
    capacity = 5 * tok_dev * top_count // (4 * experts_all)
    targets = slot_targets(routes, experts_all, capacity)
    owners = (
        jnp.full((experts_all * capacity,), tok_dev, jnp.int32)
        .at[targets]
        .set(jnp.arange(tok_dev * top_count, dtype=jnp.int32) // top_count)
    )
    padded = jnp.concatenate(
        [normed_own, jnp.zeros((1, normed_own.shape[1]), jnp.bfloat16)], axis=0
    )
    outgoing = padded[owners].reshape(sp_count, exp_dev, capacity, normed_own.shape[1])
    rows_all = lax.all_gather(
        lax.all_to_all(outgoing, "sp", split_axis=0, concat_axis=0, tiled=True),
        "tp",
        axis=3,
        tiled=True,
    )
    gate_part = jnp.einsum(
        "secd,edf->secf", rows_all, expert_gate, preferred_element_type=jnp.float32
    )
    up_part = jnp.einsum("secd,edf->secf", rows_all, expert_up, preferred_element_type=jnp.float32)
    hidden = silu_gate(gate_part, up_part).astype(jnp.bfloat16)
    hidden_all = lax.all_gather(hidden, "tp", axis=3, tiled=True)
    produced = jnp.einsum(
        "secf,efd->secd", hidden_all, expert_down, preferred_element_type=jnp.float32
    ).astype(jnp.bfloat16)
    returned = lax.all_to_all(produced, "sp", split_axis=0, concat_axis=0, tiled=True)
    returned_flat = returned.reshape(experts_all * capacity, local_width)
    picked = returned_flat[targets].astype(jnp.float32).reshape(tok_dev, top_count, local_width)
    routed = jnp.sum(picked * route_weight[:, :, None], axis=1)
    return (mid_wide + shared_out + routed).astype(jnp.bfloat16)


def solution(mesh):
    placed = (
        P("sp", "tp"),
        P("sp", "tp"),
        P("sp", "tp"),
        P("sp", "tp"),
        P("sp", "tp"),
        P(None, "tp"),
        P(),
        P("sp", None),
        P("sp", None),
        P("sp", None, "tp"),
        P("sp", None, "tp"),
        P("sp", None, "tp"),
        P(None, "tp"),
        P(None, "tp"),
        P(None, "tp"),
    )
    return jax.shard_map(
        shards, mesh=mesh, in_specs=placed, out_specs=P("sp", "tp"), check_vma=False
    )
```

profile of v0, /device:TPU:0, one launch (start us, length us, event | category | flops | bytes accessed | tf_op | source)
XLA Modules:
  0.0 383.8 jit_solution(4985606902853403032)
XLA Ops:
  6.5 1.9 copy.36
  8.6 1.8 copy.34
  11.8 15.9 %all_gather.25 = f32[4096,4]{0,1:T(4,128)S(1)} all-gather(f32[512,4]{0,1:T(4,128)S(1)} %copy-done.9), channel_id=1, replica_groups=mesh['sp'=8,'tp'=4] {'sp'}, dimensions={0}, use_global_device_ids=true | all-gather | bytes 73728 | tf_op jit(solution)/shard_map/all_gather | solution.py:55
  27.7 13.3 %all-gather.9.cloned.1.call-done = bf16[4096,4,64]{0,2,1:T(8,128)(2,1)} async-done(((bf16[512,4,64]{0,2,1:T(8,128)(2,1)}), bf16[4096,4,64]{0,2,1:T(8,128)(2,1)}) %all-gather.9.cloned.1.call-update) | async-done | bytes 2097168 | tf_op jit(solution)/shard_map/all_gather | solution.py:64
  41.0 3.2 copy.57
  44.2 27.0 %all-gather.7.cloned.1.call-done = bf16[4096,4,64]{0,2,1:T(8,128)(2,1)} async-done(((bf16[512,4,64]{0,2,1:T(8,128)(2,1)}), bf16[4096,4,64]{0,2,1:T(8,128)(2,1)}) %all-gather.7.cloned.1.call-update) | async-done | bytes 2097168 | tf_op jit(solution)/shard_map/all_gather | solution.py:63
  71.3 3.2 copy.58
  74.6 16.6 %while.17 = (s32[]{:T(128)}, f32[4,512]{1,0:T(4,128)S(1)}, f32[4,512]{1,0:T(4,128)S(1)}, f32[4,512,64]{1,2,0:T(8,128)S(1)}, s32[8]{0:T(128)S(1)}, /*index=5*/s32...) while((s32[]{:T(128)}, f32[4,512]{1,0:T(4,128)S(1)}, ...), condition=%wide.region_5.6_spmd.clone, body=%wide.region_0.5_spmd.clone.sunk | while | flops 286790656 | bytes 15676785 | solution.py:102
  75.8 6.3 %conditional.3 = ((f32[4,512]{1,0:T(4,128)S(1)}, f32[4,512]{1,0:T(4,128)S(1)}, f32[4,512,64]{1,2,0:T(8,128)S(1)})) conditional(s32[]{:T(128)} %convert_element_type.105, (f32[4,512]{1,0:T(4,128)S(1)}, f32[4,512]{1,0:T(4,128)S(1)}, f32[4,512,64]{1,2,0:T(8,128)S(1)}) %tuple.50, (s32[]{:T(128)}, s32[]{:T(128)}, bf16[8,512,4,64]{1,3,2,0:T(8,128)(2,1)}, ...), branch_computations={%region_1.1_spmd, %region_2.4_spmd} | conditional | flops 286790656 | bytes 15674446 | solution.py:99
  76.2 2.2 fusion.2
  78.4 1.4 fusion.6
  79.8 2.3 fusion.10
  92.0 9.0 %reduce-window.6 = s32[32,8,128]{2,1,0:T(8,128)S(1)} reduce-window(s32[32,8,128]{2,1,0:T(8,128)S(1)} %fusion.56, s32[]{:T(128)} %constant.93.clone.1), window={size=1x1x128 pad=0_0x0_0x127_0}, to_apply=%region_8.9 | reduce-window | flops 4161536 | bytes 262148 | tf_op jit(solution)/shard_map/reduce-window
  101.9 4.3 %scatter_custom_fusion = s32[1280]{0:T(1024)S(1)} fusion(s32[1024]{0:T(1024)S(1)} %bitcast.129, s32[1024]{0:T(1024)S(1)} %add_select_fusion, s32[]{:T(128)} %constant.98.clone.1), kind=kCustom, calls=%fused_computation.75 | custom fusion | bytes 5124 | tf_op jit(solution)/shard_map/scatter | solution.py:141
  107.0 54.9 %all-gather.11.cloned.1.call-done = bf16[512,1024]{0,1:T(8,128)(2,1)} async-done(((bf16[512,256]{0,1:T(8,128)(2,1)}), bf16[512,1024]{0,1:T(8,128)(2,1)}) %all-gather.11.cloned.1.call-update) | async-done | bytes 1048592 | tf_op jit(solution)/shard_map/all_gather | solution.py:108
  161.9 2.5 fusion.50
  164.4 8.9 %psum.7 = f32[512]{0:T(512)S(1)} all-reduce(f32[512]{0:T(512)S(1)} %get-tuple-element.335), channel_id=1, replica_groups=mesh['sp'=8,'tp'=4] {'tp'}, use_global_device_ids=true, to_apply=%region_7.8 | all-reduce | flops 512 | bytes 4096 | tf_op jit(solution)/shard_map/psum | solution.py:115
  173.6 4.7 %gather_fusion = bf16[1280,512]{1,0:T(8,128)(2,1)} fusion(bf16[513,512]{1,0:T(8,128)(2,1)S(1)} %concatenate.3, s32[2048]{0:T(1024)S(1)} %pad_clamp_fusion), kind=kCustom, calls=%fused_computation | custom fusion | bytes 2626560 | tf_op jit(solution)/shard_map/gather | solution.py:146
  178.4 36.8 %all_to_all.10 = bf16[8,4,40,512]{3,2,1,0:T(8,128)(2,1)S(1)} all-to-all(bf16[8,4,40,512]{3,2,1,0:T(8,128)(2,1)} %bitcast.116), channel_id=1, replica_groups=mesh['sp'=8,'tp'=4] {'sp'}, dimensions={0} | all-to-all | bytes 2621440 | tf_op jit(solution)/shard_map/all_to_all | solution.py:148
  216.6 59.0 %all-gather.15.cloned.1.call-done = bf16[8,4,40,2048]{3,2,0,1:T(8,128)(2,1)} async-done(((bf16[8,4,40,512]{3,2,0,1:T(8,128)(2,1)}), bf16[8,4,40,2048]{3,2,0,1:T(8,128)(2,1)}) %all-gather.15.cloned.1.call-update) | async-done | bytes 5242896 | tf_op jit(solution)/shard_map/all_gather | solution.py:147
  275.7 4.8 %fusion.37 = f32[8,4,40,128]{3,2,0,1:T(8,128)S(1)} fusion(bf16[8,4,40,2048]{3,2,0,1:T(8,128)(2,1)} %all-gather.15.cloned.1.call-done, bf16[4,2048,128]{2,1,0:T(8,128)(2,1)} %param.28), kind=kOutput, calls=%fused_computation.48 | convolution fusion | flops 671088640 | bytes 7995392 | tf_op jit(solution)/shard_map/secd,edf->secf/dot_general | solution.py:153
  281.0 2.3 fusion.46
  283.9 28.1 %all-gather.17.cloned.1.call-done = bf16[8,4,40,512]{3,2,0,1:T(8,128)(2,1)} async-done(((bf16[8,4,40,128]{3,2,0,1:T(8,128)(2,1)}), bf16[8,4,40,512]{3,2,0,1:T(8,128)(2,1)}) %all-gather.17.cloned.1.call-update) | async-done | bytes 1310736 | tf_op jit(solution)/shard_map/all_gather | solution.py:158
  312.0 2.2 fusion.31
  315.3 4.6 %all-to-all-start.1 = ((bf16[8,4,40,512]{3,2,1,0:T(8,128)(2,1)}), bf16[8,4,40,512]{3,2,1,0:T(8,128)(2,1)S(1)}, u32[]{:S(2)}, u32[]{:S(2)}) async-start(bf16[8,4,40,512]{3,2,1,0:T(8,128)(2,1)} %copy.45), calls=%async_computation.1 | async-start | bytes 2621440 | tf_op jit(solution)/shard_map/all_to_all | solution.py:162
  320.8 27.9 %all-gather.13.cloned.1.call-done = bf16[512,2048]{1,0:T(8,128)(2,1)} async-done(((bf16[512,512]{1,0:T(8,128)(2,1)}), bf16[512,2048]{1,0:T(8,128)(2,1)}) %all-gather.13.cloned.1.call-update) | async-done | bytes 2097168 | tf_op jit(solution)/shard_map/all_gather | solution.py:121
  348.7 2.5 fusion.62
  352.0 10.6 %all_gather.29 = bf16[512,512]{1,0:T(8,128)(2,1)} all-gather(bf16[512,128]{1,0:T(8,128)(2,1)S(1)} %fusion.49), channel_id=1, replica_groups=mesh['sp'=8,'tp'=4] {'tp'}, dimensions={1}, use_global_device_ids=true | all-gather | bytes 655360 | tf_op jit(solution)/shard_map/all_gather | solution.py:128
  362.6 5.1 %gather_fusion.1 = bf16[1024,512]{1,0:T(8,128)(2,1)} fusion(bf16[1280,512]{1,0:T(8,128)(2,1)S(1)} %bitcast.115, s32[1024]{0:T(1024)S(1)} %broadcast_clamp_fusion), kind=kCustom, calls=%fused_computation.1 | custom fusion | bytes 2101248 | tf_op jit(solution)/shard_map/gather | solution.py:164
  367.7 3.4 reshape.124
  371.1 4.5 %multiply_reduce_fusion = f32[512,512]{1,0:T(8,128)S(1)} fusion(f32[512,2,512]{2,1,0:T(2,128)} %reshape.124, f32[512,2]{1,0:T(8,128)S(1)} %copy-done.7), kind=kLoop, calls=%fused_computation.38 | loop fusion | flops 786432 | bytes 3149824 | tf_op jit(solution)/shard_map/reduce_sum | solution.py:165
  375.7 1.2 fusion.36
  (105 shorter events, 14.6 us)
Async XLA Ops:
  6.5 305.4 %copy-start = (bf16[4,512,512]{2,1,0:T(8,128)(2,1)S(1)}, bf16[4,512,512]{2,1,0:T(8,128)(2,1)}, u32[]{:S(2)}) copy-start(bf16[4,512,512]{2,1,0:T(8,128)(2,1)} %param.30) | copy-start | bytes 6291460
  6.5 5.1 %copy-start.10 = (bf16[512,256]{1,0:T(8,128)(2,1)S(1)}, bf16[512,256]{1,0:T(8,128)(2,1)}, u32[]{:S(2)}) copy-start(bf16[512,256]{1,0:T(8,128)(2,1)} %param.19) | copy-start | bytes 786436
  6.5 5.2 %copy-start.9 = (f32[512,4]{0,1:T(4,128)S(1)}, f32[512,4]{0,1:T(4,128)}, u32[]{:S(2)}) copy-start(f32[512,4]{0,1:T(4,128)} %param.22) | copy-start | bytes 24580
  6.5 34.5 %all-gather.9.cloned.1.call-start = ((), (), s32[]{:S(2)}) async-start(), calls=%async_computation.3 | async-start | bytes 2359296 | tf_op jit(solution)/shard_map/all_gather | solution.py:64
  8.5 62.8 %all-gather.7.cloned.1.call-start = ((), (), s32[]{:S(2)}) async-start(), calls=%async_computation.2 | async-start | bytes 2359296 | tf_op jit(solution)/shard_map/all_gather | solution.py:63
  10.4 151.5 %all-gather.11.cloned.1.call-start = ((), (), s32[]{:S(2)}) async-start(), calls=%async_computation.4 | async-start | bytes 1310720 | tf_op jit(solution)/shard_map/all_gather | solution.py:108
  74.6 26.8 %copy-start.11 = (s32[512,2]{0,1:T(2,128)S(1)}, s32[512,2]{0,1:T(2,128)}, u32[]{:S(2)}) copy-start(s32[512,2]{0,1:T(2,128)} %param.26) | copy-start | bytes 12292
  92.0 183.7 %all-gather.15.cloned.1.call-start = ((), (), s32[]{:S(2)}) async-start(), calls=%async_computation.6 | async-start | bytes 6553600 | tf_op jit(solution)/shard_map/all_gather | solution.py:147
  164.4 9.2 %copy-start.5 = (bf16[512,512]{1,0:T(8,128)(2,1)}, bf16[512,512]{1,0:T(8,128)(2,1)S(1)}, u32[]{:S(2)}) copy-start(bf16[512,512]{1,0:T(8,128)(2,1)S(1)} %get-tuple-element.336) | copy-start | bytes 1572868
  173.6 4.8 %copy-start.2 = (bf16[512,512]{1,0:T(8,128)(2,1)}, bf16[512,512]{1,0:T(8,128)(2,1)S(1)}, u32[]{:S(2)}) copy-start(bf16[512,512]{1,0:T(8,128)(2,1)S(1)} %fusion.52) | copy-start | bytes 1572868
  216.4 95.6 %all-gather.17.cloned.1.call-start = ((), (), s32[]{:S(2)}) async-start(), calls=%async_computation.7 | async-start | bytes 1638400 | tf_op jit(solution)/shard_map/all_gather | solution.py:158
  275.7 4.8 %copy-start.1 = (bf16[8,4,40,2048]{3,2,0,1:T(8,128)(2,1)S(1)}, bf16[8,4,40,2048]{3,2,0,1:T(8,128)(2,1)}, u32[]{:S(2)}) copy-start(bf16[8,4,40,2048]{3,2,0,1:T(8,128)(2,1)} %all-gather.15.cloned.1.call-done) | copy-start | bytes 15728644
  275.7 5.3 %copy-start.13 = (bf16[4,2048,128]{2,1,0:T(8,128)(2,1)S(1)}, bf16[4,2048,128]{2,1,0:T(8,128)(2,1)}, u32[]{:S(2)}) copy-start(bf16[4,2048,128]{2,1,0:T(8,128)(2,1)} %param.29) | copy-start | bytes 6291460
  283.3 65.4 %all-gather.13.cloned.1.call-start = ((), (), s32[]{:S(2)}) async-start(), calls=%async_computation.5 | async-start | bytes 2621440 | tf_op jit(solution)/shard_map/all_gather | solution.py:121
  314.1 5.8 %copy-start.12 = (f32[512,2]{0,1:T(2,128)S(1)}, f32[512,2]{0,1:T(2,128)}, u32[]{:S(2)}) copy-start(f32[512,2]{0,1:T(2,128)} %param.27) | copy-start | bytes 12292
  315.3 47.3 %all-to-all-start.1 = ((bf16[8,4,40,512]{3,2,1,0:T(8,128)(2,1)}), bf16[8,4,40,512]{3,2,1,0:T(8,128)(2,1)S(1)}, u32[]{:S(2)}, u32[]{:S(2)}) async-start(bf16[8,4,40,512]{3,2,1,0:T(8,128)(2,1)} %copy.45), calls=%async_computation.1 | async-start | bytes 2621440 | tf_op jit(solution)/shard_map/all_to_all | solution.py:162
  348.7 2.5 copy-start.3
  348.7 2.5 copy-start.14
  367.7 3.4 copy-start.7
  371.1 4.5 %copy-start.4 = (bf16[512,512]{1,0:T(8,128)(2,1)S(1)}, bf16[512,512]{1,0:T(8,128)(2,1)}, u32[]{:S(2)}) copy-start(bf16[512,512]{1,0:T(8,128)(2,1)} %all_gather.29) | copy-start | bytes 1572868
  371.1 4.5 %copy-start.6 = (bf16[512,512]{1,0:T(8,128)(2,1)S(1)}, bf16[512,512]{1,0:T(8,128)(2,1)}, u32[]{:S(2)}) copy-start(bf16[512,512]{1,0:T(8,128)(2,1)} %copy-done.5) | copy-start | bytes 1572868
  371.1 4.6 %copy-start.8 = (bf16[512,512]{1,0:T(8,128)(2,1)S(1)}, bf16[512,512]{1,0:T(8,128)(2,1)}, u32[]{:S(2)}) copy-start(bf16[512,512]{1,0:T(8,128)(2,1)} %param.33) | copy-start | bytes 1572868
Sparse Core Ops, SparseCore 0:
  8.9 32.0 all-gather.8
  42.6 28.6 all-gather.6
  92.1 69.7 all-gather.10
  216.5 59.1 all-gather.14
  283.4 28.5 all-gather.16
  313.6 35.0 all-gather.12
where the time goes:
time: 385 us; the launch traced here: 384 us
  waiting for transfers between devices  211 us (55%)
  blocking collectives  72.3 us (19%)
  local copies, waits for them, and re-layouts  38.3 us (10%)
  matrix products  20.8 us (5%)
  other arithmetic  17.1 us (4%)
  between operations  13.8 us (4%)
  loops' own time  5.65 us (1%)
  starting transfers between devices  4.99 us (1%)
    all_gather x1, waiting for transfers between devices, shards(): lax.all_gather(lax.all_to_all(outgoing, 'sp', split_axis=0, concat_axis=0...  59 us
    all_gather x1, waiting for transfers between devices, shards(): lax.all_gather(attended, 'tp', axis=1, tiled=True)  54.9 us
    all_to_all x1, blocking collectives, shards(): lax.all_to_all(outgoing, 'sp', split_axis=0, concat_axis=0, tiled=True)  36.8 us
    all_gather x1, waiting for transfers between devices, shards(): hidden_all = lax.all_gather(hidden, 'tp', axis=3, tiled=True)  28.1 us
    all_gather x1, waiting for transfers between devices, shards(): normed = lax.all_gather(normed_own, 'tp', axis=1, tiled=True)  27.9 us
    all_gather x1, waiting for transfers between devices, shards(): key_part = lax.all_gather(key_heads, 'sp', axis=0, tiled=True)  27 us
    all_gather x1, blocking collectives, shards(): all_gates = lax.all_gather(log_gate_sums, 'sp', axis=0, tiled=True)  15.9 us
    all_gather x1, waiting for transfers between devices, shards(): value_part = lax.all_gather(value_heads, 'sp', axis=0, tiled=True)  13.3 us
  transfers between devices with their start and end apart: 7, of which 6 were waited for; matrix products, arithmetic and copies ran while one was open for 7% of the time, Pallas kernels for 0%

commit v1 on v0

--- a/solution.py
+++ b/solution.py
@@ -60,8 +60,11 @@
     )
     key_heads = key_vectors.reshape(tok_dev, local_heads, head_dim)
     value_heads = value_vectors.reshape(tok_dev, local_heads, head_dim)
-    key_part = lax.all_gather(key_heads, "sp", axis=0, tiled=True)
-    value_part = lax.all_gather(value_heads, "sp", axis=0, tiled=True)
+    key_part, value_part = jnp.split(
+        lax.all_gather(jnp.concatenate([key_heads, value_heads], axis=1), "sp", axis=0, tiled=True),
+        [key_heads.shape[1]],
+        axis=1,
+    )
     part_rows = key_part.shape[0]
     block_size = math.gcd(part_rows, 512)
     key_blocks = key_part.reshape(part_rows // block_size, block_size, local_heads, head_dim)

time: 385 us -> 374 us (0.971)
  waiting for transfers between devices: 211 us -> 203 us
    all_gather x2 -> x1, waiting for transfers between devices: 40.3 us -> 33.3 us  [shards(): lax.all_gather(jnp.concatenate([key_heads, value_heads], axis=1), 'sp', a...]
    reshape x2 -> x0, local copies, waits for them, and re-layouts: 6.41 us -> none  [the longest x1 3.21 us: shards(): value_part.reshape(part_rows // block_size, block_size, local_heads, head...]
  transfers between devices with their start and end apart: 7 -> 6, of which waited for: 6 -> 5; matrix products, arithmetic and copies ran while one was open for 7% -> 6% of each run, Pallas kernels for 0% -> 0%
where the time goes in v1:
time: 374 us; the launch traced here: 373 us
  waiting for transfers between devices  203 us (54%)
  blocking collectives  72.1 us (19%)
  local copies, waits for them, and re-layouts  35 us (9%)
  matrix products  20.8 us (6%)
  other arithmetic  17.9 us (5%)
  between operations  13.5 us (4%)
  loops' own time  5.65 us (2%)
  starting transfers between devices  4.98 us (1%)
    all_gather x1, waiting for transfers between devices, shards(): lax.all_gather(lax.all_to_all(outgoing, 'sp', split_axis=0, concat_axis=0...  59 us
    all_gather x1, waiting for transfers between devices, shards(): lax.all_gather(attended, 'tp', axis=1, tiled=True)  54.2 us
    all_to_all x1, blocking collectives, shards(): lax.all_to_all(outgoing, 'sp', split_axis=0, concat_axis=0, tiled=True)  36.8 us
    all_gather x1, waiting for transfers between devices, shards(): lax.all_gather(jnp.concatenate([key_heads, value_heads], axis=1), 'sp', a...  33.3 us
    all_gather x1, waiting for transfers between devices, shards(): hidden_all = lax.all_gather(hidden, 'tp', axis=3, tiled=True)  28.1 us
    all_gather x1, waiting for transfers between devices, shards(): normed = lax.all_gather(normed_own, 'tp', axis=1, tiled=True)  27.9 us
    all_gather x1, blocking collectives, shards(): all_gates = lax.all_gather(log_gate_sums, 'sp', axis=0, tiled=True)  15.8 us
    all_gather x1, blocking collectives, shards(): lax.all_gather(shared_mid, 'tp', axis=1, tiled=True)  10.6 us
  transfers between devices with their start and end apart: 6, of which 5 were waited for; matrix products, arithmetic and copies ran while one was open for 6% of the time, Pallas kernels for 0%

profile of v1, /device:TPU:0, one launch (start us, length us, event | category | flops | bytes accessed | tf_op | source)
XLA Modules:
  0.0 373.1 jit_solution(18007078552913371516)
XLA Ops:
  6.6 1.2 copy.34
  10.5 15.8 %all_gather.22 = f32[4096,4]{0,1:T(4,128)S(1)} all-gather(f32[512,4]{0,1:T(4,128)S(1)} %copy-done.9), channel_id=1, replica_groups=mesh['sp'=8,'tp'=4] {'sp'}, dimensions={0}, use_global_device_ids=true | all-gather | bytes 73728 | tf_op jit(solution)/shard_map/all_gather | solution.py:55
  26.3 33.3 %all-gather.6.cloned.1.call-done = bf16[4096,8,64]{0,2,1:T(8,128)(2,1)} async-done(((bf16[512,8,64]{0,2,1:T(8,128)(2,1)}), bf16[4096,8,64]{0,2,1:T(8,128)(2,1)}) %all-gather.6.cloned.1.call-update) | async-done | bytes 4194320 | tf_op jit(solution)/shard_map/all_gather | solution.py:64
  59.6 2.7 fusion.62
  62.3 2.5 copy_bitcast_fusion
  64.9 16.6 %while.17 = (s32[]{:T(128)}, f32[4,512]{1,0:T(4,128)S(1)}, f32[4,512]{1,0:T(4,128)S(1)}, f32[4,512,64]{1,2,0:T(8,128)S(1)}, s32[8]{0:T(128)S(1)}, /*index=5*/s32...) while((s32[]{:T(128)}, f32[4,512]{1,0:T(4,128)S(1)}, ...), condition=%wide.region_5.6_spmd.clone, body=%wide.region_0.5_spmd.clone.sunk | while | flops 286790656 | bytes 15676785 | solution.py:105
  66.2 6.3 %conditional.3 = ((f32[4,512]{1,0:T(4,128)S(1)}, f32[4,512]{1,0:T(4,128)S(1)}, f32[4,512,64]{1,2,0:T(8,128)S(1)})) conditional(s32[]{:T(128)} %convert_element_type.105, (f32[4,512]{1,0:T(4,128)S(1)}, f32[4,512]{1,0:T(4,128)S(1)}, f32[4,512,64]{1,2,0:T(8,128)S(1)}) %tuple.52, (s32[]{:T(128)}, s32[]{:T(128)}, bf16[8,512,4,64]{1,3,2,0:T(8,128)(2,1)}, ...), branch_computations={%region_1.1_spmd, %region_2.4_spmd} | conditional | flops 286790656 | bytes 15674446 | solution.py:102
  66.5 2.2 fusion.2
  68.8 1.4 fusion.6
  70.1 2.3 fusion.10
  82.4 9.0 %reduce-window.6 = s32[32,8,128]{2,1,0:T(8,128)S(1)} reduce-window(s32[32,8,128]{2,1,0:T(8,128)S(1)} %fusion.56, s32[]{:T(128)} %constant.93.clone.1), window={size=1x1x128 pad=0_0x0_0x127_0}, to_apply=%region_8.9 | reduce-window | flops 4161536 | bytes 262148 | tf_op jit(solution)/shard_map/reduce-window
  92.3 4.3 %scatter_custom_fusion = s32[1280]{0:T(1024)S(1)} fusion(s32[1024]{0:T(1024)S(1)} %bitcast.125, s32[1024]{0:T(1024)S(1)} %add_select_fusion, s32[]{:T(128)} %constant.98.clone.1), kind=kCustom, calls=%fused_computation.76 | custom fusion | bytes 5124 | tf_op jit(solution)/shard_map/scatter | solution.py:144
  97.4 54.2 %all-gather.8.cloned.1.call-done = bf16[512,1024]{0,1:T(8,128)(2,1)} async-done(((bf16[512,256]{0,1:T(8,128)(2,1)}), bf16[512,1024]{0,1:T(8,128)(2,1)}) %all-gather.8.cloned.1.call-update) | async-done | bytes 1048592 | tf_op jit(solution)/shard_map/all_gather | solution.py:111
  151.6 2.5 fusion.50
  154.1 8.9 %psum.7 = f32[512]{0:T(512)S(1)} all-reduce(f32[512]{0:T(512)S(1)} %get-tuple-element.337), channel_id=1, replica_groups=mesh['sp'=8,'tp'=4] {'tp'}, use_global_device_ids=true, to_apply=%region_7.8 | all-reduce | flops 512 | bytes 4096 | tf_op jit(solution)/shard_map/psum | solution.py:118
  163.3 4.7 %gather_fusion = bf16[1280,512]{1,0:T(8,128)(2,1)} fusion(bf16[513,512]{1,0:T(8,128)(2,1)S(1)} %concatenate.7, s32[2048]{0:T(1024)S(1)} %pad_clamp_fusion), kind=kCustom, calls=%fused_computation | custom fusion | bytes 2626560 | tf_op jit(solution)/shard_map/gather | solution.py:149
  168.1 36.8 %all_to_all.10 = bf16[8,4,40,512]{3,2,1,0:T(8,128)(2,1)S(1)} all-to-all(bf16[8,4,40,512]{3,2,1,0:T(8,128)(2,1)} %bitcast.116), channel_id=1, replica_groups=mesh['sp'=8,'tp'=4] {'sp'}, dimensions={0} | all-to-all | bytes 2621440 | tf_op jit(solution)/shard_map/all_to_all | solution.py:151
  204.8 1.2 copy.44
  206.3 59.0 %all-gather.12.cloned.1.call-done = bf16[8,4,40,2048]{3,2,0,1:T(8,128)(2,1)} async-done(((bf16[8,4,40,512]{3,2,0,1:T(8,128)(2,1)}), bf16[8,4,40,2048]{3,2,0,1:T(8,128)(2,1)}) %all-gather.12.cloned.1.call-update) | async-done | bytes 5242896 | tf_op jit(solution)/shard_map/all_gather | solution.py:150
  265.4 4.8 %fusion.37 = f32[8,4,40,128]{3,2,0,1:T(8,128)S(1)} fusion(bf16[8,4,40,2048]{3,2,0,1:T(8,128)(2,1)} %all-gather.12.cloned.1.call-done, bf16[4,2048,128]{2,1,0:T(8,128)(2,1)} %param.28), kind=kOutput, calls=%fused_computation.48 | convolution fusion | flops 671088640 | bytes 7995392 | tf_op jit(solution)/shard_map/secd,edf->secf/dot_general | solution.py:156
  270.7 2.3 fusion.46
  273.6 28.1 %all-gather.14.cloned.1.call-done = bf16[8,4,40,512]{3,2,0,1:T(8,128)(2,1)} async-done(((bf16[8,4,40,128]{3,2,0,1:T(8,128)(2,1)}), bf16[8,4,40,512]{3,2,0,1:T(8,128)(2,1)}) %all-gather.14.cloned.1.call-update) | async-done | bytes 1310736 | tf_op jit(solution)/shard_map/all_gather | solution.py:161
  301.7 2.2 fusion.31
  303.8 1.2 copy.45
  305.0 4.6 %all-to-all-start.1 = ((bf16[8,4,40,512]{3,2,1,0:T(8,128)(2,1)}), bf16[8,4,40,512]{3,2,1,0:T(8,128)(2,1)S(1)}, u32[]{:S(2)}, u32[]{:S(2)}) async-start(bf16[8,4,40,512]{3,2,1,0:T(8,128)(2,1)} %copy.45), calls=%async_computation.1 | async-start | bytes 2621440 | tf_op jit(solution)/shard_map/all_to_all | solution.py:165
  310.5 27.9 %all-gather.10.cloned.1.call-done = bf16[512,2048]{1,0:T(8,128)(2,1)} async-done(((bf16[512,512]{1,0:T(8,128)(2,1)}), bf16[512,2048]{1,0:T(8,128)(2,1)}) %all-gather.10.cloned.1.call-update) | async-done | bytes 2097168 | tf_op jit(solution)/shard_map/all_gather | solution.py:124
  338.4 2.5 fusion.63
  341.7 10.6 %all_gather.25 = bf16[512,512]{1,0:T(8,128)(2,1)} all-gather(bf16[512,128]{1,0:T(8,128)(2,1)S(1)} %fusion.49), channel_id=1, replica_groups=mesh['sp'=8,'tp'=4] {'tp'}, dimensions={1}, use_global_device_ids=true | all-gather | bytes 655360 | tf_op jit(solution)/shard_map/all_gather | solution.py:131
  352.3 5.1 %gather_fusion.1 = bf16[1024,512]{1,0:T(8,128)(2,1)} fusion(bf16[1280,512]{1,0:T(8,128)(2,1)S(1)} %bitcast.113, s32[1024]{0:T(1024)S(1)} %broadcast_clamp_fusion), kind=kCustom, calls=%fused_computation.1 | custom fusion | bytes 2101248 | tf_op jit(solution)/shard_map/gather | solution.py:167
  357.4 3.4 reshape.124
  360.8 4.5 %multiply_reduce_fusion = f32[512,512]{1,0:T(8,128)S(1)} fusion(f32[512,2,512]{2,1,0:T(2,128)} %reshape.124, f32[512,2]{1,0:T(8,128)S(1)} %copy-done.7), kind=kLoop, calls=%fused_computation.38 | loop fusion | flops 786432 | bytes 3149824 | tf_op jit(solution)/shard_map/reduce_sum | solution.py:168
  365.3 1.2 fusion.36
  (103 shorter events, 13.4 us)
Async XLA Ops:
  6.5 295.1 %copy-start = (bf16[4,512,512]{2,1,0:T(8,128)(2,1)S(1)}, bf16[4,512,512]{2,1,0:T(8,128)(2,1)}, u32[]{:S(2)}) copy-start(bf16[4,512,512]{2,1,0:T(8,128)(2,1)} %param.30) | copy-start | bytes 6291460
  6.5 3.3 copy-start.11
  6.5 3.8 %copy-start.10 = (bf16[512,256]{1,0:T(8,128)(2,1)S(1)}, bf16[512,256]{1,0:T(8,128)(2,1)}, u32[]{:S(2)}) copy-start(bf16[512,256]{1,0:T(8,128)(2,1)} %param.19) | copy-start | bytes 786436
  6.5 4.0 %copy-start.9 = (f32[512,4]{0,1:T(4,128)S(1)}, f32[512,4]{0,1:T(4,128)}, u32[]{:S(2)}) copy-start(f32[512,4]{0,1:T(4,128)} %param.22) | copy-start | bytes 24580
  6.5 53.1 %all-gather.6.cloned.1.call-start = ((), (), s32[]{:S(2)}) async-start(), calls=%async_computation.2 | async-start | bytes 4718592 | tf_op jit(solution)/shard_map/all_gather | solution.py:64
  9.8 141.8 %all-gather.8.cloned.1.call-start = ((), (), s32[]{:S(2)}) async-start(), calls=%async_computation.3 | async-start | bytes 1310720 | tf_op jit(solution)/shard_map/all_gather | solution.py:111
  82.3 183.1 %all-gather.12.cloned.1.call-start = ((), (), s32[]{:S(2)}) async-start(), calls=%async_computation.5 | async-start | bytes 6553600 | tf_op jit(solution)/shard_map/all_gather | solution.py:150
  154.1 9.2 %copy-start.5 = (bf16[512,512]{1,0:T(8,128)(2,1)}, bf16[512,512]{1,0:T(8,128)(2,1)S(1)}, u32[]{:S(2)}) copy-start(bf16[512,512]{1,0:T(8,128)(2,1)S(1)} %get-tuple-element.338) | copy-start | bytes 1572868
  163.3 4.8 %copy-start.2 = (bf16[512,512]{1,0:T(8,128)(2,1)}, bf16[512,512]{1,0:T(8,128)(2,1)S(1)}, u32[]{:S(2)}) copy-start(bf16[512,512]{1,0:T(8,128)(2,1)S(1)} %fusion.52) | copy-start | bytes 1572868
  206.1 95.6 %all-gather.14.cloned.1.call-start = ((), (), s32[]{:S(2)}) async-start(), calls=%async_computation.6 | async-start | bytes 1638400 | tf_op jit(solution)/shard_map/all_gather | solution.py:161
  265.4 4.8 %copy-start.1 = (bf16[8,4,40,2048]{3,2,0,1:T(8,128)(2,1)S(1)}, bf16[8,4,40,2048]{3,2,0,1:T(8,128)(2,1)}, u32[]{:S(2)}) copy-start(bf16[8,4,40,2048]{3,2,0,1:T(8,128)(2,1)} %all-gather.12.cloned.1.call-done) | copy-start | bytes 15728644
  265.4 5.3 %copy-start.13 = (bf16[4,2048,128]{2,1,0:T(8,128)(2,1)S(1)}, bf16[4,2048,128]{2,1,0:T(8,128)(2,1)}, u32[]{:S(2)}) copy-start(bf16[4,2048,128]{2,1,0:T(8,128)(2,1)} %param.29) | copy-start | bytes 6291460
  273.0 65.4 %all-gather.10.cloned.1.call-start = ((), (), s32[]{:S(2)}) async-start(), calls=%async_computation.4 | async-start | bytes 2621440 | tf_op jit(solution)/shard_map/all_gather | solution.py:124
  303.8 5.8 %copy-start.12 = (f32[512,2]{0,1:T(2,128)S(1)}, f32[512,2]{0,1:T(2,128)}, u32[]{:S(2)}) copy-start(f32[512,2]{0,1:T(2,128)} %param.27) | copy-start | bytes 12292
  305.0 47.3 %all-to-all-start.1 = ((bf16[8,4,40,512]{3,2,1,0:T(8,128)(2,1)}), bf16[8,4,40,512]{3,2,1,0:T(8,128)(2,1)S(1)}, u32[]{:S(2)}, u32[]{:S(2)}) async-start(bf16[8,4,40,512]{3,2,1,0:T(8,128)(2,1)} %copy.45), calls=%async_computation.1 | async-start | bytes 2621440 | tf_op jit(solution)/shard_map/all_to_all | solution.py:165
  338.4 2.5 copy-start.3
  338.4 2.6 copy-start.14
  357.4 3.4 copy-start.7
  360.8 4.5 %copy-start.4 = (bf16[512,512]{1,0:T(8,128)(2,1)S(1)}, bf16[512,512]{1,0:T(8,128)(2,1)}, u32[]{:S(2)}) copy-start(bf16[512,512]{1,0:T(8,128)(2,1)} %all_gather.25) | copy-start | bytes 1572868
  360.8 4.5 %copy-start.6 = (bf16[512,512]{1,0:T(8,128)(2,1)S(1)}, bf16[512,512]{1,0:T(8,128)(2,1)}, u32[]{:S(2)}) copy-start(bf16[512,512]{1,0:T(8,128)(2,1)} %copy-done.5) | copy-start | bytes 1572868
  360.8 4.6 %copy-start.8 = (bf16[512,512]{1,0:T(8,128)(2,1)S(1)}, bf16[512,512]{1,0:T(8,128)(2,1)}, u32[]{:S(2)}) copy-start(bf16[512,512]{1,0:T(8,128)(2,1)} %param.33) | copy-start | bytes 1572868
Sparse Core Ops, SparseCore 0:
  9.9 49.6 all-gather.5
  82.4 69.1 all-gather.7
  206.2 59.1 all-gather.11
  273.1 28.5 all-gather.13
  303.3 35.0 all-gather.9
